TPU v7x, 256 devices: a whole 4x4x8 slice. The times are simulated.
256 devices in a mesh: sp: 64 (over z, y, core), tp: 4 (over x).
Axes of the slice: x: 4, y: 4, z: 8, core: 2. Of those that a mesh axis runs over, the one named last changes fastest.
Arguments:
- residual: bfloat16 [65536, 2048], P(('sp', 'tp')), may hold values from -6 to 6
- pool_input: bfloat16 [65536, 1024], P('sp', 'tp'), may hold values from -6 to 6
- doc_ids: int32 [65536], P('sp'), may hold values from 0 to 31, never falling along the last dimension, each value on 1 to 4096 neighbouring positions
- pool_map: bfloat16 [4, 256, 256], P('tp'), may hold values from -0.375 to 0.375
- pool_scale: float32 [1024], P('tp'), may hold values from 0.1 to 1.9
- out_weight: bfloat16 [1024, 2048], replicated, may hold values from -0.1875 to 0.1875
- mix_gain: float32 [2048], replicated, may hold values from 0.1 to 1.9
- mix_shift: float32 [2048], replicated, may hold values from -1.75 to 1.75
- group_router: bfloat16 [2048, 4], replicated, may hold values from -0.125 to 0.125
- expert_router: bfloat16 [2048, 64], replicated, may hold values from -0.125 to 0.125
- expert_gate: bfloat16 [64, 2048, 512], P('sp'), may hold values from -0.375 to 0.375
- expert_up: bfloat16 [64, 2048, 512], P('sp'), may hold values from -0.375 to 0.375
- expert_down: bfloat16 [64, 512, 2048], P('sp'), may hold values from -0.75 to 0.75
- routes: int32 [65536, 2], P(('sp', 'tp')), may hold values from 0 to 63, as said below
- ffn_gain: float32 [2048], replicated, may hold values from 0.1 to 1.9
- ffn_shift: float32 [2048], replicated, may hold values from -1.75 to 1.75
Outputs:
- layer_out: bfloat16 [65536, 2048], P(('sp', 'tp'))
Inputs may be any that keep to these rules, and one draw needn't show every extreme that they name: `doc_ids`: document numbers never fall along the positions; each document has 1 to 4096 positions. `routes`: A token names 2 different experts. In each aligned block of half of one device's 256 rows, 32 experts are named exactly 8 times each and the others not at all.
All inputs are finite; a program needn't handle non-finite values.
Results may differ from a plain program's by a relative error of at most 0.0073.
Values may be sent and summed in bfloat16 or wider, within the bound.
No kernel may reach another device: no remote copies, remote signals or barrier semaphores. Data moves between devices by JAX's collectives and lax.ppermute only.
A program may use at most 128 MiB of HBM per device.

v0:
```python
import jax
import jax.numpy as jnp
from jax import lax
from jax.sharding import PartitionSpec as P

skip_scale = 2.0**0.5
epsilon = 1e-05


def from_behind(block, axis, distance):
    devices = range(lax.axis_size(axis))
    route = [(i - distance, i) for i in devices if i - distance in devices]
    return lax.ppermute(block, axis, route)


def layer_norm(values, norm_gain, norm_shift):
    center = values - jnp.mean(values, axis=-1, keepdims=True)
    spread = jnp.mean(center * center, axis=-1, keepdims=True)
    return center * lax.rsqrt(spread + epsilon) * norm_gain + norm_shift


def route_weights(normed, chosen, group_router, expert_router):
    group_logits = jnp.dot(normed, group_router, preferred_element_type=jnp.float32)
    expert_logits = jnp.dot(normed, expert_router, preferred_element_type=jnp.float32)
    group_count = group_logits.shape[1]
    expert_count = expert_logits.shape[1]
    group_exp = jnp.exp(group_logits)
    group_prob = group_exp / jnp.sum(group_exp, axis=1, keepdims=True)
    expert_ids = jnp.arange(expert_count, dtype=jnp.int32)
    picked = jnp.sum(
        jnp.where(chosen[:, :, None] == expert_ids[None, None, :], expert_logits[:, None, :], 0.0),
        axis=2,
    )
    picked_exp = jnp.exp(picked)
    pair_share = picked_exp / jnp.sum(picked_exp, axis=1, keepdims=True)
    group_of = chosen // (expert_count // group_count)
    group_ids = jnp.arange(group_count, dtype=jnp.int32)
    group_share = jnp.sum(
        jnp.where(group_of[:, :, None] == group_ids[None, None, :], group_prob[:, None, :], 0.0),
        axis=2,
    )
    return group_share * pair_share


def expert_ffn(arrived, expert_gate, expert_up, expert_down):
    sources, slot_count, width = arrived.shape
    gathered = arrived.reshape(sources * slot_count, width)
    gate_out = jnp.dot(gathered, expert_gate[0], preferred_element_type=jnp.float32)
    up_out = jnp.dot(gathered, expert_up[0], preferred_element_type=jnp.float32)
    hidden = (jax.nn.silu(gate_out) * up_out).astype(jnp.bfloat16)
    result = jnp.dot(hidden, expert_down[0], preferred_element_type=jnp.float32).astype(
        jnp.bfloat16
    )
    return result.reshape(sources, slot_count, width)


def fill_slots(normed, chosen, capacity, expert_count):
    flat_routes = chosen.reshape(-1)
    entry_count = flat_routes.shape[0]
    onehot = (flat_routes[:, None] == jnp.arange(expert_count, dtype=jnp.int32)[None, :]).astype(
        jnp.int32
    )
    slot_rank = jnp.sum((jnp.cumsum(onehot, axis=0) - onehot) * onehot, axis=1)
    slot_index = flat_routes * capacity + slot_rank
    token_ids = jnp.arange(entry_count, dtype=jnp.int32) // chosen.shape[1]
    source_row = (
        jnp.full((expert_count * capacity,), normed.shape[0], jnp.int32)
        .at[slot_index]
        .set(token_ids)
    )
    padded = jnp.concatenate([normed, jnp.zeros((1, normed.shape[1]), normed.dtype)], axis=0)
    outgoing = jnp.take(padded, source_row, axis=0).reshape(expert_count, capacity, normed.shape[1])
    return (outgoing, slot_index)


def combine_rows(returned, slot_index, weight):
    flat_out = returned.reshape(-1, returned.shape[2])
    picked = jnp.take(flat_out, slot_index, axis=0).reshape(
        weight.shape[0], weight.shape[1], flat_out.shape[1]
    )
    return jnp.sum(weight[:, :, None] * picked.astype(jnp.float32), axis=1)


def on_device(
    residual,
    pool_input,
    doc_ids,
    pool_map,
    pool_scale,
    out_weight,
    mix_gain,
    mix_shift,
    group_router,
    expert_router,
    expert_gate,
    expert_up,
    expert_down,
    routes,
    ffn_gain,
    ffn_shift,
):
    seq_rows = pool_input.shape[0]
    reach_rows = 15
    expert_count = lax.axis_size("sp")
    tp_count = lax.axis_size("tp")
    window = jnp.left_shift(jnp.int32(2), lax.axis_index("tp"))
    first_row = lax.axis_index("sp") * seq_rows
    tail_values, tail_docs = from_behind(
        (pool_input[seq_rows - reach_rows :], doc_ids[seq_rows - reach_rows :]), "sp", 1
    )
    source = jnp.concatenate([tail_values, pool_input], axis=0).astype(jnp.float32)
    all_docs = jnp.concatenate([tail_docs, doc_ids], axis=0)
    positions = first_row - reach_rows + jnp.arange(seq_rows + reach_rows, dtype=jnp.int32)
    running = jnp.zeros((seq_rows, source.shape[1]), jnp.float32)
    weight_sum = jnp.zeros((seq_rows, 1), jnp.float32)
    for offset in range(reach_rows + 1):
        begin_row = reach_rows - offset
        earlier = source[begin_row : begin_row + seq_rows]
        keep_mask = (
            (all_docs[begin_row : begin_row + seq_rows] == doc_ids)
            & (positions[begin_row : begin_row + seq_rows] >= 0)
            & (offset < window)
        )
        same_doc = keep_mask.astype(jnp.float32)[:, None]
        running = running + same_doc * earlier
        weight_sum = weight_sum + same_doc
    pooled = (running / weight_sum - source[reach_rows:]).astype(jnp.bfloat16)
    mixed = (jnp.dot(pooled, pool_map[0], preferred_element_type=jnp.float32) * pool_scale).astype(
        jnp.bfloat16
    )
    row_count = seq_rows // tp_count
    blocks = mixed.reshape(tp_count, row_count, mixed.shape[1])
    branch = jnp.einsum(
        "abc,cd->abd",
        lax.all_to_all(blocks, "tp", split_axis=0, concat_axis=2, tiled=True),
        out_weight,
        preferred_element_type=jnp.float32,
    )[0]
    normed = layer_norm(
        skip_scale * residual.astype(jnp.float32) + branch, mix_gain, mix_shift
    ).astype(jnp.bfloat16)
    weight = route_weights(normed, routes, group_router, expert_router)
    half_most = row_count * routes.shape[1] // expert_count
    half_rows = row_count // 2
    routed_parts = []
    for piece_index in range(2):
        rows_here = slice(piece_index * half_rows, (piece_index + 1) * half_rows)
        outgoing, slot_index = fill_slots(
            normed[rows_here], routes[rows_here], half_most, expert_count
        )
        returned = lax.all_to_all(
            expert_ffn(
                lax.all_to_all(outgoing, "sp", split_axis=0, concat_axis=0, tiled=True),
                expert_gate,
                expert_up,
                expert_down,
            ),
            "sp",
            split_axis=0,
            concat_axis=0,
            tiled=True,
        )
        routed_parts.append(combine_rows(returned, slot_index, weight[rows_here]))
    routed = jnp.concatenate(routed_parts, axis=0)
    return layer_norm(skip_scale * normed.astype(jnp.float32) + routed, ffn_gain, ffn_shift).astype(
        jnp.bfloat16
    )


def solution(mesh):
    in_specs = (
        P(("sp", "tp"), None),
        P("sp", "tp"),
        P("sp"),
        P("tp", None, None),
        P("tp"),
        P(),
        P(),
        P(),
        P(),
        P(),
        P("sp", None, None),
        P("sp", None, None),
        P("sp", None, None),
        P(("sp", "tp"), None),
        P(),
        P(),
    )
    out_specs = P(("sp", "tp"), None)
    return jax.shard_map(
        on_device, mesh=mesh, in_specs=in_specs, out_specs=out_specs, check_vma=False
    )
```

profile of v0, /device:TPU:8, one launch (start us, length us, event | category | flops | bytes accessed | tf_op | source)
XLA Modules:
  0.0 301.4 jit_solution(417035532456568899)
XLA Ops:
  0.0 0.9 slice.180
  0.9 1.9 collective-permute-start
  2.8 0.8 slice.182
  3.5 3.6 %collective-permute-start.1 = (s32[15]{0:T(128)S(1)}, s32[15]{0:T(128)S(1)}, u32[]{:S(2)}, u32[]{:S(2)}) collective-permute-start(s32[15]{0:T(128)S(1)} %slice.182), channel_id=1, source_target_pairs={{0,4},{4,8},{8,12},{12,16},{16,20},{20,24},{24,28},{28,32},{32,36}... | collective-permute-start | bytes 188 | tf_op jit(solution)/shard_map/ppermute | solution.py:13
  7.1 0.7 fusion.172
  7.8 0.1 copy.41
  7.9 0.1 eq.150
  8.1 0.1 eq.154
  8.3 0.1 copy.44
  8.4 0.1 mul.304
  8.6 0.6 reduce-window.16
  9.2 0.2 slice_reduce_fusion
  9.5 1.4 scatter_custom_fusion.1
  10.9 1.4 add_add_fusion
  12.4 1.2 maximum_convert_fusion
  13.6 4.4 %fusion.26 = bf16[1024,256]{1,0:T(8,128)(2,1)S(1)} fusion(f32[256]{0:T(256)S(1)} %copy-done.14, f32[1039,256]{1,0:T(8,128)S(1)} %maximum_convert_fusion, f32[1024]{0:T(1024)S(1)} %get-tuple-element.11, f32[1024]{0:T(1024)S(1)} %get-tuple-element.27, f32[1024]{0:T(1024)S(1)} %get-tuple-element.26, f32[1024]{0:T(1024)S(1)} %get-tuple-element.25, ...), kind=kOutput, calls=%fused_computation.37 | convolution fusion | flops 143654912 | bytes 17503232 | tf_op jit(solution)/shard_map/dot_general | solution.py:128
  18.0 1.0 copy.34
  19.0 4.3 %all-to-all-start = ((bf16[4,256,256]{1,2,0:T(8,128)(2,1)}), bf16[4,256,256]{1,2,0:T(8,128)(2,1)S(1)}, u32[]{:S(2)}, u32[]{:S(2)}) async-start(bf16[4,256,256]{1,2,0:T(8,128)(2,1)} %copy.34), calls=%async_computation | async-start | bytes 1048576 | tf_op jit(solution)/shard_map/all_to_all | solution.py:135
  23.3 9.6 %all-to-all-done = bf16[4,256,256]{1,2,0:T(8,128)(2,1)S(1)} async-done(((bf16[4,256,256]{1,2,0:T(8,128)(2,1)}), bf16[4,256,256]{1,2,0:T(8,128)(2,1)S(1)}, u32[]{:S(2)}, u32[]{:S(2)}) %all-to-all-start) | async-done | bytes 524320 | tf_op jit(solution)/shard_map/all_to_all | solution.py:135
  32.9 3.8 %fusion.173 = (f32[256]{0:T(256)S(1)}, f32[256,2048]{1,0:T(8,128)S(1)}) fusion(bf16[256,1024]{0,1:T(8,128)(2,1)S(1)} %bitcast.116, bf16[1024,2048]{1,0:T(8,128)(2,1)} %param.25, bf16[256,2048]{1,0:T(8,128)(2,1)} %param.20), kind=kOutput, calls=%fused_computation.265 | convolution fusion | flops 1075838720 | bytes 7865344 | tf_op jit(solution)/shard_map/abc,cd->abd/dot_general | solution.py:133
  36.8 0.4 multiply_reduce_fusion.3
  37.2 0.3 copy-done.6
  37.6 0.5 add_convert_fusion.1
  38.0 0.1 copy-done.1
  38.2 0.9 copy-done.3
  39.2 3.3 %gather_fusion.2 = bf16[512,2048]{1,0:T(8,128)(2,1)} fusion(bf16[129,2048]{1,0:T(8,128)(2,1)S(1)} %concatenate.18, s32[1024]{0:T(1024)S(1)} %pad_clamp_fusion.1), kind=kCustom, calls=%fused_computation.2.clone | custom fusion | bytes 4196352 | tf_op jit(solution)/shard_map/jit(_take)/gather | solution.py:72
  42.5 3.2 %select_bitcast_fusion = bf16[64,8,2048]{2,1,0:T(8,128)(2,1)} fusion(bf16[512,2048]{1,0:T(8,128)(2,1)} %gather_fusion.2, pred[512]{0:T(512)(128)(4,1)S(1)} %compare_and_fusion.1), kind=kLoop, calls=%fused_computation.26 | loop fusion | flops 1048576 | bytes 4194816 | tf_op jit(solution)/shard_map/reshape | solution.py:72
  45.6 12.1 %all-to-all-start.3 = ((bf16[64,8,2048]{2,1,0:T(8,128)(2,1)}), bf16[64,8,2048]{2,1,0:T(8,128)(2,1)}, u32[]{:S(2)}, u32[]{:S(2)}) async-start(bf16[64,8,2048]{2,1,0:T(8,128)(2,1)} %select_bitcast_fusion), calls=%async_computation.3 | async-start | bytes 4194304 | tf_op jit(solution)/shard_map/all_to_all | solution.py:153
  57.8 0.1 copy.36
  57.9 0.1 eq.142
  58.0 0.1 eq.146
  58.2 0.1 copy.39
  58.3 0.1 mul.296
  58.4 0.6 reduce-window.14
  59.1 0.2 slice_reduce_fusion.1
  59.4 1.4 scatter_custom_fusion
  60.9 1.2 slice_select_fusion
  62.0 3.3 %gather_fusion = bf16[512,2048]{1,0:T(8,128)(2,1)} fusion(bf16[129,2048]{1,0:T(8,128)(2,1)S(1)} %slice_select_fusion, s32[1024]{0:T(1024)S(1)} %pad_clamp_fusion.3), kind=kCustom, calls=%fused_computation.clone | custom fusion | bytes 4196352 | tf_op jit(solution)/shard_map/jit(_take)/gather | solution.py:72
  65.3 3.2 %select_bitcast_fusion.1 = bf16[64,8,2048]{2,1,0:T(8,128)(2,1)} fusion(bf16[512,2048]{1,0:T(8,128)(2,1)} %gather_fusion, pred[512]{0:T(512)(128)(4,1)S(1)} %compare_and_fusion.3), kind=kLoop, calls=%fused_computation.27 | loop fusion | flops 1048576 | bytes 4194816 | tf_op jit(solution)/shard_map/reshape | solution.py:72
  68.6 40.4 %all-to-all-done.3 = bf16[64,8,2048]{2,1,0:T(8,128)(2,1)} async-done(((bf16[64,8,2048]{2,1,0:T(8,128)(2,1)}), bf16[64,8,2048]{2,1,0:T(8,128)(2,1)}, u32[]{:S(2)}, u32[]{:S(2)}) %all-to-all-start.3) | async-done | bytes 2097184 | tf_op jit(solution)/shard_map/all_to_all | solution.py:153
  108.9 5.6 %all-to-all-start.1 = ((bf16[64,8,2048]{2,1,0:T(8,128)(2,1)}), bf16[64,8,2048]{2,1,0:T(8,128)(2,1)}, u32[]{:S(2)}, u32[]{:S(2)}) async-start(bf16[64,8,2048]{2,1,0:T(8,128)(2,1)} %select_bitcast_fusion.1), calls=%async_computation.1 | async-start | bytes 4194304 | tf_op jit(solution)/shard_map/all_to_all | solution.py:153
  114.6 3.5 %fusion.4 = f32[512,512]{1,0:T(8,128)S(1)} fusion(bf16[64,8,2048]{2,1,0:T(8,128)(2,1)} %all-to-all-done.3, bf16[1,2048,512]{2,1,0:T(8,128)(2,1)} %param.30), kind=kOutput, calls=%fused_computation.14 | convolution fusion | flops 1073741824 | bytes 5242880 | tf_op jit(solution)/shard_map/dot_general | solution.py:48
  118.1 6.0 %fusion.1 = bf16[64,8,2048]{2,1,0:T(8,128)(2,1)} fusion(bf16[1,512,2048]{2,1,0:T(8,128)(2,1)S(1)} %copy-done, bf16[1,2048,512]{2,1,0:T(8,128)(2,1)} %param.31, bf16[64,8,2048]{2,1,0:T(8,128)(2,1)} %all-to-all-done.3, f32[512,512]{1,0:T(8,128)S(1)} %fusion.4), kind=kOutput, calls=%fused_computation.9 | convolution fusion | flops 2150105088 | bytes 9437184 | tf_op jit(solution)/shard_map/dot_general | solution.py:51
  124.1 41.6 %all-to-all-done.1 = bf16[64,8,2048]{2,1,0:T(8,128)(2,1)} async-done(((bf16[64,8,2048]{2,1,0:T(8,128)(2,1)}), bf16[64,8,2048]{2,1,0:T(8,128)(2,1)}, u32[]{:S(2)}, u32[]{:S(2)}) %all-to-all-start.1) | async-done | bytes 2097184 | tf_op jit(solution)/shard_map/all_to_all | solution.py:153
  165.7 5.6 %all-to-all-start.4 = ((bf16[64,8,2048]{2,1,0:T(8,128)(2,1)}), bf16[64,8,2048]{2,1,0:T(8,128)(2,1)}, u32[]{:S(2)}, u32[]{:S(2)}) async-start(bf16[64,8,2048]{2,1,0:T(8,128)(2,1)} %fusion.1), calls=%async_computation.4 | async-start | bytes 4194304 | tf_op jit(solution)/shard_map/all_to_all | solution.py:151
  171.3 3.5 %fusion.12 = f32[512,512]{1,0:T(8,128)S(1)} fusion(bf16[1,2048,512]{2,1,0:T(8,128)(2,1)} %param.30, bf16[64,8,2048]{2,1,0:T(8,128)(2,1)} %all-to-all-done.1), kind=kOutput, calls=%fused_computation.22 | convolution fusion | flops 1073741824 | bytes 5242880 | tf_op jit(solution)/shard_map/dot_general | solution.py:48
  174.8 6.0 %fusion = bf16[64,8,2048]{2,1,0:T(8,128)(2,1)} fusion(bf16[1,512,2048]{2,1,0:T(8,128)(2,1)S(1)} %copy-done, bf16[1,2048,512]{2,1,0:T(8,128)(2,1)} %param.31, bf16[64,8,2048]{2,1,0:T(8,128)(2,1)} %all-to-all-done.1, f32[512,512]{1,0:T(8,128)S(1)} %fusion.12), kind=kOutput, calls=%fused_computation.8 | convolution fusion | flops 2150105088 | bytes 9437184 | tf_op jit(solution)/shard_map/dot_general | solution.py:51
  180.8 41.7 %all-to-all-done.4 = bf16[64,8,2048]{2,1,0:T(8,128)(2,1)} async-done(((bf16[64,8,2048]{2,1,0:T(8,128)(2,1)}), bf16[64,8,2048]{2,1,0:T(8,128)(2,1)}, u32[]{:S(2)}, u32[]{:S(2)}) %all-to-all-start.4) | async-done | bytes 2097184 | tf_op jit(solution)/shard_map/all_to_all | solution.py:151
  222.5 5.6 %all-to-all-start.2 = ((bf16[64,8,2048]{2,1,0:T(8,128)(2,1)}), bf16[64,8,2048]{2,1,0:T(8,128)(2,1)}, u32[]{:S(2)}, u32[]{:S(2)}) async-start(bf16[64,8,2048]{2,1,0:T(8,128)(2,1)} %fusion), calls=%async_computation.2 | async-start | bytes 4194304 | tf_op jit(solution)/shard_map/all_to_all | solution.py:151
  228.2 0.4 fusion.175
  228.8 0.4 fusion.174
  229.2 0.1 copy.40
  229.3 0.1 copy.35
  229.5 4.2 %gather_fusion.3 = bf16[256,2048]{1,0:T(8,128)(2,1)S(1)} fusion(bf16[512,2048]{1,0:T(8,128)(2,1)} %bitcast.21, s32[1024]{0:T(1024)S(1)} %pad_clamp_fusion), kind=kCustom, calls=%fused_computation.3.clone | custom fusion | bytes 2098176 | tf_op jit(solution)/shard_map/jit(_take)/gather | solution.py:78
  233.7 1.6 select_convert_fusion
  235.3 3.5 %reshape.223 = f32[128,2,2048]{2,1,0:T(2,128)} reshape(f32[256,2048]{1,0:T(8,128)} %select_convert_fusion) | data formatting | bytes 4194304 | tf_op jit(solution)/shard_map/convert_element_type | solution.py:81
  238.8 40.5 %all-to-all-done.2 = bf16[64,8,2048]{2,1,0:T(8,128)(2,1)} async-done(((bf16[64,8,2048]{2,1,0:T(8,128)(2,1)}), bf16[64,8,2048]{2,1,0:T(8,128)(2,1)}, u32[]{:S(2)}, u32[]{:S(2)}) %all-to-all-start.2) | async-done | bytes 2097184 | tf_op jit(solution)/shard_map/all_to_all | solution.py:151
  279.3 4.2 %gather_fusion.1 = bf16[256,2048]{1,0:T(8,128)(2,1)S(1)} fusion(bf16[512,2048]{1,0:T(8,128)(2,1)} %bitcast.14, s32[1024]{0:T(1024)S(1)} %pad_clamp_fusion.2), kind=kCustom, calls=%fused_computation.1.clone | custom fusion | bytes 2098176 | tf_op jit(solution)/shard_map/jit(_take)/gather | solution.py:78
  283.5 1.6 select_convert_fusion.1
  285.1 3.5 %reshape.222 = f32[128,2,2048]{2,1,0:T(2,128)} reshape(f32[256,2048]{1,0:T(8,128)} %select_convert_fusion.1) | data formatting | bytes 4194304 | tf_op jit(solution)/shard_map/convert_element_type | solution.py:81
  288.5 8.6 %multiply_reduce_fusion.1 = (f32[128,2048]{1,0:T(8,128)S(1)}, f32[128,2048]{1,0:T(8,128)S(1)}) fusion(f32[128,2,2048]{2,1,0:T(2,128)} %reshape.223, f32[128,2]{1,0:T(8,128)S(1)} %copy.40, f32[128,2,2048]{2,1,0:T(2,128)} %reshape.222, f32[128,2]{1,0:T(8,128)S(1)} %copy.35), kind=kLoop, calls=%fused_computation.30 | loop fusion | flops 1572864 | bytes 6293504 | tf_op jit(solution)/shard_map/reduce_sum | solution.py:81
  297.1 0.7 fusion.155
  297.8 0.8 multiply_reduce_fusion
  298.6 2.8 add_convert_fusion
  (64 shorter events, 0.8 us)
Async XLA Ops:
  0.0 118.0 %copy-start = (bf16[1,512,2048]{2,1,0:T(8,128)(2,1)S(1)}, bf16[1,512,2048]{2,1,0:T(8,128)(2,1)}, u32[]{:S(2)}) copy-start(bf16[1,512,2048]{2,1,0:T(8,128)(2,1)} %param.32) | copy-start | bytes 6291460
  0.0 13.5 %copy-start.14 = (f32[256]{0:T(256)S(1)}, f32[256]{0:T(256)}, u32[]{:S(2)}) copy-start(f32[256]{0:T(256)} %param.24) | copy-start | bytes 3076
  0.0 13.6 %copy-start.13 = (bf16[1,256,256]{2,1,0:T(8,128)(2,1)S(1)}, bf16[1,256,256]{2,1,0:T(8,128)(2,1)}, u32[]{:S(2)}) copy-start(bf16[1,256,256]{2,1,0:T(8,128)(2,1)} %param.23) | copy-start | bytes 393220
  0.9 11.5 %collective-permute-start = (bf16[15,256]{1,0:T(8,128)(2,1)S(1)}, bf16[15,256]{1,0:T(8,128)(2,1)S(1)}, u32[]{:S(2)}, u32[]{:S(2)}) collective-permute-start(bf16[15,256]{1,0:T(8,128)(2,1)S(1)} %slice.180), channel_id=1, source_target_pairs={{0,4},{4,8},{8,12},{12,16},{16,20},{20,24},{24,28},{28,32},{32,36}... | collective-permute-start | bytes 23048 | tf_op jit(solution)/shard_map/ppermute | solution.py:13
  3.5 7.4 %collective-permute-start.1 = (s32[15]{0:T(128)S(1)}, s32[15]{0:T(128)S(1)}, u32[]{:S(2)}, u32[]{:S(2)}) collective-permute-start(s32[15]{0:T(128)S(1)} %slice.182), channel_id=1, source_target_pairs={{0,4},{4,8},{8,12},{12,16},{16,20},{20,24},{24,28},{28,32},{32,36}... | collective-permute-start | bytes 188 | tf_op jit(solution)/shard_map/ppermute | solution.py:13
  19.0 13.9 %all-to-all-start = ((bf16[4,256,256]{1,2,0:T(8,128)(2,1)}), bf16[4,256,256]{1,2,0:T(8,128)(2,1)S(1)}, u32[]{:S(2)}, u32[]{:S(2)}) async-start(bf16[4,256,256]{1,2,0:T(8,128)(2,1)} %copy.34), calls=%async_computation | async-start | bytes 1048576 | tf_op jit(solution)/shard_map/all_to_all | solution.py:135
  36.8 1.4 copy-start.1
  36.8 0.7 copy-start.6
  36.8 0.8 copy-start.7
  38.2 1.0 copy-start.3
  45.6 15.2 %copy-start.12 = (pred[129]{0:T(512)(128)(4,1)S(1)}, pred[129]{0:T(512)(128)(4,1)}, u32[]{:S(2)}) copy-start(pred[129]{0:T(512)(128)(4,1)} %constant.119.clone.1) | copy-start | bytes 391
  45.6 63.3 %all-to-all-start.3 = ((bf16[64,8,2048]{2,1,0:T(8,128)(2,1)}), bf16[64,8,2048]{2,1,0:T(8,128)(2,1)}, u32[]{:S(2)}, u32[]{:S(2)}) async-start(bf16[64,8,2048]{2,1,0:T(8,128)(2,1)} %select_bitcast_fusion), calls=%async_computation.3 | async-start | bytes 4194304 | tf_op jit(solution)/shard_map/all_to_all | solution.py:153
  108.9 56.8 %all-to-all-start.1 = ((bf16[64,8,2048]{2,1,0:T(8,128)(2,1)}), bf16[64,8,2048]{2,1,0:T(8,128)(2,1)}, u32[]{:S(2)}, u32[]{:S(2)}) async-start(bf16[64,8,2048]{2,1,0:T(8,128)(2,1)} %select_bitcast_fusion.1), calls=%async_computation.1 | async-start | bytes 4194304 | tf_op jit(solution)/shard_map/all_to_all | solution.py:153
  165.7 56.8 %all-to-all-start.4 = ((bf16[64,8,2048]{2,1,0:T(8,128)(2,1)}), bf16[64,8,2048]{2,1,0:T(8,128)(2,1)}, u32[]{:S(2)}, u32[]{:S(2)}) async-start(bf16[64,8,2048]{2,1,0:T(8,128)(2,1)} %fusion.1), calls=%async_computation.4 | async-start | bytes 4194304 | tf_op jit(solution)/shard_map/all_to_all | solution.py:151
  180.8 47.4 %copy-start.8 = (s32[256,2]{0,1:T(2,128)S(1)}, s32[256,2]{0,1:T(2,128)}, u32[]{:S(2)}) copy-start(s32[256,2]{0,1:T(2,128)} %param.33) | copy-start | bytes 6148
  180.8 47.4 %copy-start.4 = (bf16[256,2048]{1,0:T(8,128)(2,1)S(1)}, bf16[256,2048]{1,0:T(8,128)(2,1)}, u32[]{:S(2)}) copy-start(bf16[256,2048]{1,0:T(8,128)(2,1)} %copy-done.3) | copy-start | bytes 3145732
  180.8 47.4 %copy-start.5 = (bf16[2048,64]{0,1:T(8,128)(2,1)S(1)}, bf16[2048,64]{0,1:T(8,128)(2,1)}, u32[]{:S(2)}) copy-start(bf16[2048,64]{0,1:T(8,128)(2,1)} %param.29) | copy-start | bytes 786436
  180.8 48.0 %copy-start.9 = (bf16[2048,4]{0,1:T(4,128)(2,1)S(1)}, bf16[2048,4]{0,1:T(4,128)(2,1)}, u32[]{:S(2)}) copy-start(bf16[2048,4]{0,1:T(4,128)(2,1)} %param.28) | copy-start | bytes 49156
  222.5 56.8 %all-to-all-start.2 = ((bf16[64,8,2048]{2,1,0:T(8,128)(2,1)}), bf16[64,8,2048]{2,1,0:T(8,128)(2,1)}, u32[]{:S(2)}, u32[]{:S(2)}) async-start(bf16[64,8,2048]{2,1,0:T(8,128)(2,1)} %fusion), calls=%async_computation.2 | async-start | bytes 4194304 | tf_op jit(solution)/shard_map/all_to_all | solution.py:151
  288.5 8.6 %copy-start.2 = (f32[256,2048]{1,0:T(8,128)S(1)}, f32[256,2048]{1,0:T(8,128)}, u32[]{:S(2)}) copy-start(f32[256,2048]{1,0:T(8,128)} %copy-done.1) | copy-start | bytes 6291460
  297.8 0.8 copy-start.10
  297.8 0.8 copy-start.11
where the time goes:
time: 302 us; the launch traced here: 301 us
  waiting for transfers between devices  174 us (58%)
  starting transfers between devices  38.8 us (13%)
  local copies, waits for them, and re-layouts  30.8 us (10%)
  other arithmetic  29.4 us (10%)
  matrix products  28 us (9%)
    all_to_all x2, waiting for transfers between devices, on_device(): lax.all_to_all(expert_ffn(lax.all_to_all(outgoing, 'sp', split_axis=0, co...  82.2 us
    all_to_all x2, waiting for transfers between devices, on_device(): lax.all_to_all(outgoing, 'sp', split_axis=0, concat_axis=0, tiled=True)  82 us
    all_to_all x2, starting transfers between devices, on_device(): lax.all_to_all(outgoing, 'sp', split_axis=0, concat_axis=0, tiled=True)  17.8 us
    dot_general x2, matrix products, expert_ffn(): jnp.dot(hidden, expert_down[0], preferred_element_type=jnp.float32)  12 us
    all_to_all x2, starting transfers between devices, on_device(): lax.all_to_all(expert_ffn(lax.all_to_all(outgoing, 'sp', split_axis=0, co...  11.3 us
    all_to_all x1, waiting for transfers between devices, on_device(): lax.all_to_all(blocks, 'tp', split_axis=0, concat_axis=2, tiled=True)  9.63 us
    reduce_sum x1, other arithmetic, combine_rows(): return jnp.sum(weight[:, :, None] * picked.astype(jnp.float32), axis=1)  8.57 us
    gather x2, local copies, waits for them, and re-layouts, combine_rows(): jnp.take(flat_out, slot_index, axis=0)  8.45 us
  transfers between devices with their start and end apart: 7, of which 5 were waited for; matrix products, arithmetic and copies ran while one was open for 15% of the time, Pallas kernels for 0%

commit v1 on v0

--- a/solution.py
+++ b/solution.py
@@ -2,9 +2,17 @@
 import jax.numpy as jnp
 from jax import lax
 from jax.sharding import PartitionSpec as P
+from jax.lax import all_to_all, axis_size
 
 skip_scale = 2.0**0.5
 epsilon = 1e-05
+
+
+def slots_remake(point):
+    aux = jnp.concatenate(
+        all_to_all(jnp.stack(jnp.split(point, axis_size("tp"), axis=0)), "tp", 0, 0), axis=2
+    )
+    return aux
 
 
 def from_behind(block, axis, distance):
@@ -131,10 +139,7 @@
     row_count = seq_rows // tp_count
     blocks = mixed.reshape(tp_count, row_count, mixed.shape[1])
     branch = jnp.einsum(
-        "abc,cd->abd",
-        lax.all_to_all(blocks, "tp", split_axis=0, concat_axis=2, tiled=True),
-        out_weight,
-        preferred_element_type=jnp.float32,
+        "abc,cd->abd", slots_remake(blocks), out_weight, preferred_element_type=jnp.float32
     )[0]
     normed = layer_norm(
         skip_scale * residual.astype(jnp.float32) + branch, mix_gain, mix_shift

time: 302 us -> 303 us (level)
  no operation moved by 1% of the time
where the time goes in v1:
time: 303 us; the launch traced here: 302 us
  waiting for transfers between devices  174 us (57%)
  starting transfers between devices  38.8 us (13%)
  other arithmetic  30.3 us (10%)
  local copies, waits for them, and re-layouts  30.1 us (10%)
  matrix products  28 us (9%)
    all_to_all x2, waiting for transfers between devices, on_device(): lax.all_to_all(expert_ffn(lax.all_to_all(outgoing, 'sp', split_axis=0, co...  82.2 us
    all_to_all x2, waiting for transfers between devices, on_device(): lax.all_to_all(outgoing, 'sp', split_axis=0, concat_axis=0, tiled=True)  82 us
    all_to_all x2, starting transfers between devices, on_device(): lax.all_to_all(outgoing, 'sp', split_axis=0, concat_axis=0, tiled=True)  17.8 us
    dot_general x2, matrix products, expert_ffn(): jnp.dot(hidden, expert_down[0], preferred_element_type=jnp.float32)  12 us
    all_to_all x2, starting transfers between devices, on_device(): lax.all_to_all(expert_ffn(lax.all_to_all(outgoing, 'sp', split_axis=0, co...  11.3 us
    all_to_all x1, waiting for transfers between devices, slots_remake(): all_to_all(jnp.stack(jnp.split(point, axis_size('tp'), axis=0)), 'tp', 0, 0)  9.63 us
    reduce_sum x1, other arithmetic, combine_rows(): return jnp.sum(weight[:, :, None] * picked.astype(jnp.float32), axis=1)  8.57 us
    gather x2, local copies, waits for them, and re-layouts, combine_rows(): jnp.take(flat_out, slot_index, axis=0)  8.45 us
  transfers between devices with their start and end apart: 7, of which 5 were waited for; matrix products, arithmetic and copies ran while one was open for 15% of the time, Pallas kernels for 0%

profile of v1, /device:TPU:8, one launch (start us, length us, event | category | flops | bytes accessed | tf_op | source)
XLA Modules:
  0.0 301.6 jit_solution(10519891241765402545)
XLA Ops:
  0.0 0.9 slice.184
  0.9 1.9 collective-permute-start
  2.8 0.8 slice.186
  3.5 3.6 %collective-permute-start.1 = (s32[15]{0:T(128)S(1)}, s32[15]{0:T(128)S(1)}, u32[]{:S(2)}, u32[]{:S(2)}) collective-permute-start(s32[15]{0:T(128)S(1)} %slice.186), channel_id=1, source_target_pairs={{0,4},{4,8},{8,12},{12,16},{16,20},{20,24},{24,28},{28,32},{32,36}... | collective-permute-start | bytes 188 | tf_op jit(solution)/shard_map/ppermute | solution.py:21
  7.1 0.7 fusion.172
  7.8 0.1 copy.41
  7.9 0.1 eq.150
  8.1 0.1 eq.154
  8.3 0.1 copy.44
  8.4 0.1 mul.304
  8.6 0.6 reduce-window.16
  9.2 0.2 slice_reduce_fusion
  9.5 1.4 scatter_custom_fusion.1
  10.9 1.4 add_add_fusion
  12.4 1.2 maximum_convert_fusion
  13.6 4.4 %fusion.26 = bf16[1024,256]{1,0:T(8,128)(2,1)S(1)} fusion(f32[256]{0:T(256)S(1)} %copy-done.14, f32[1039,256]{1,0:T(8,128)S(1)} %maximum_convert_fusion, f32[1024]{0:T(1024)S(1)} %get-tuple-element.11, f32[1024]{0:T(1024)S(1)} %get-tuple-element.27, f32[1024]{0:T(1024)S(1)} %get-tuple-element.26, f32[1024]{0:T(1024)S(1)} %get-tuple-element.25, ...), kind=kOutput, calls=%fused_computation.37 | convolution fusion | flops 143654912 | bytes 17503232 | tf_op jit(solution)/shard_map/dot_general | solution.py:136
  18.1 0.9 pad_maximum_fusion
  18.9 4.3 %all-to-all-start = ((bf16[4,1,256,256]{3,2,1,0:T(8,128)(2,1)}), bf16[4,1,256,256]{3,2,1,0:T(8,128)(2,1)S(1)}, u32[]{:S(2)}, u32[]{:S(2)}) async-start(bf16[4,1,256,256]{3,2,1,0:T(8,128)(2,1)} %pad_maximum_fusion), calls=%async_computation | async-start | bytes 1048576 | tf_op jit(solution)/shard_map/all_to_all | solution.py:13
  23.2 9.6 %all-to-all-done = bf16[4,1,256,256]{3,2,1,0:T(8,128)(2,1)S(1)} async-done(((bf16[4,1,256,256]{3,2,1,0:T(8,128)(2,1)}), bf16[4,1,256,256]{3,2,1,0:T(8,128)(2,1)S(1)}, u32[]{:S(2)}, u32[]{:S(2)}) %all-to-all-start) | async-done | bytes 524320 | tf_op jit(solution)/shard_map/all_to_all | solution.py:13
  32.9 0.2 copy.34
  33.1 3.8 %fusion.173 = (f32[256]{0:T(256)S(1)}, f32[256,2048]{1,0:T(8,128)S(1)}) fusion(bf16[256,1024]{0,1:T(8,128)(2,1)S(1)} %bitcast.120, bf16[1024,2048]{1,0:T(8,128)(2,1)} %param.25, bf16[256,2048]{1,0:T(8,128)(2,1)} %param.20), kind=kOutput, calls=%fused_computation.270 | convolution fusion | flops 1075838720 | bytes 7865344 | tf_op jit(solution)/shard_map/abc,cd->abd/dot_general | solution.py:141
  37.0 0.4 multiply_reduce_fusion.3
  37.3 0.3 copy-done.6
  37.7 0.5 add_convert_fusion.1
  38.2 0.1 copy-done.1
  38.3 0.9 copy-done.3
  39.3 3.3 %gather_fusion.2 = bf16[512,2048]{1,0:T(8,128)(2,1)} fusion(bf16[129,2048]{1,0:T(8,128)(2,1)S(1)} %concatenate.18, s32[1024]{0:T(1024)S(1)} %pad_clamp_fusion.1), kind=kCustom, calls=%fused_computation.2.clone | custom fusion | bytes 4196352 | tf_op jit(solution)/shard_map/jit(_take)/gather | solution.py:80
  42.6 3.2 %select_bitcast_fusion = bf16[64,8,2048]{2,1,0:T(8,128)(2,1)} fusion(bf16[512,2048]{1,0:T(8,128)(2,1)} %gather_fusion.2, pred[512]{0:T(512)(128)(4,1)S(1)} %compare_and_fusion.1), kind=kLoop, calls=%fused_computation.26 | loop fusion | flops 1048576 | bytes 4194816 | tf_op jit(solution)/shard_map/reshape | solution.py:80
  45.8 12.1 %all-to-all-start.3 = ((bf16[64,8,2048]{2,1,0:T(8,128)(2,1)}), bf16[64,8,2048]{2,1,0:T(8,128)(2,1)}, u32[]{:S(2)}, u32[]{:S(2)}) async-start(bf16[64,8,2048]{2,1,0:T(8,128)(2,1)} %select_bitcast_fusion), calls=%async_computation.3 | async-start | bytes 4194304 | tf_op jit(solution)/shard_map/all_to_all | solution.py:158
  57.9 0.1 copy.36
  58.0 0.1 eq.142
  58.2 0.1 eq.146
  58.3 0.1 copy.39
  58.4 0.1 mul.296
  58.6 0.6 reduce-window.14
  59.2 0.2 slice_reduce_fusion.1
  59.5 1.4 scatter_custom_fusion
  61.0 1.2 slice_select_fusion
  62.2 3.3 %gather_fusion = bf16[512,2048]{1,0:T(8,128)(2,1)} fusion(bf16[129,2048]{1,0:T(8,128)(2,1)S(1)} %slice_select_fusion, s32[1024]{0:T(1024)S(1)} %pad_clamp_fusion.3), kind=kCustom, calls=%fused_computation.clone | custom fusion | bytes 4196352 | tf_op jit(solution)/shard_map/jit(_take)/gather | solution.py:80
  65.5 3.2 %select_bitcast_fusion.1 = bf16[64,8,2048]{2,1,0:T(8,128)(2,1)} fusion(bf16[512,2048]{1,0:T(8,128)(2,1)} %gather_fusion, pred[512]{0:T(512)(128)(4,1)S(1)} %compare_and_fusion.3), kind=kLoop, calls=%fused_computation.27 | loop fusion | flops 1048576 | bytes 4194816 | tf_op jit(solution)/shard_map/reshape | solution.py:80
  68.7 40.4 %all-to-all-done.3 = bf16[64,8,2048]{2,1,0:T(8,128)(2,1)} async-done(((bf16[64,8,2048]{2,1,0:T(8,128)(2,1)}), bf16[64,8,2048]{2,1,0:T(8,128)(2,1)}, u32[]{:S(2)}, u32[]{:S(2)}) %all-to-all-start.3) | async-done | bytes 2097184 | tf_op jit(solution)/shard_map/all_to_all | solution.py:158
  109.1 5.6 %all-to-all-start.1 = ((bf16[64,8,2048]{2,1,0:T(8,128)(2,1)}), bf16[64,8,2048]{2,1,0:T(8,128)(2,1)}, u32[]{:S(2)}, u32[]{:S(2)}) async-start(bf16[64,8,2048]{2,1,0:T(8,128)(2,1)} %select_bitcast_fusion.1), calls=%async_computation.1 | async-start | bytes 4194304 | tf_op jit(solution)/shard_map/all_to_all | solution.py:158
  114.7 3.5 %fusion.4 = f32[512,512]{1,0:T(8,128)S(1)} fusion(bf16[64,8,2048]{2,1,0:T(8,128)(2,1)} %all-to-all-done.3, bf16[1,2048,512]{2,1,0:T(8,128)(2,1)} %param.30), kind=kOutput, calls=%fused_computation.14 | convolution fusion | flops 1073741824 | bytes 5242880 | tf_op jit(solution)/shard_map/dot_general | solution.py:56
  118.2 6.0 %fusion.1 = bf16[64,8,2048]{2,1,0:T(8,128)(2,1)} fusion(bf16[1,512,2048]{2,1,0:T(8,128)(2,1)S(1)} %copy-done, bf16[1,2048,512]{2,1,0:T(8,128)(2,1)} %param.31, bf16[64,8,2048]{2,1,0:T(8,128)(2,1)} %all-to-all-done.3, f32[512,512]{1,0:T(8,128)S(1)} %fusion.4), kind=kOutput, calls=%fused_computation.9 | convolution fusion | flops 2150105088 | bytes 9437184 | tf_op jit(solution)/shard_map/dot_general | solution.py:59
  124.2 41.7 %all-to-all-done.1 = bf16[64,8,2048]{2,1,0:T(8,128)(2,1)} async-done(((bf16[64,8,2048]{2,1,0:T(8,128)(2,1)}), bf16[64,8,2048]{2,1,0:T(8,128)(2,1)}, u32[]{:S(2)}, u32[]{:S(2)}) %all-to-all-start.1) | async-done | bytes 2097184 | tf_op jit(solution)/shard_map/all_to_all | solution.py:158
  165.9 5.6 %all-to-all-start.4 = ((bf16[64,8,2048]{2,1,0:T(8,128)(2,1)}), bf16[64,8,2048]{2,1,0:T(8,128)(2,1)}, u32[]{:S(2)}, u32[]{:S(2)}) async-start(bf16[64,8,2048]{2,1,0:T(8,128)(2,1)} %fusion.1), calls=%async_computation.4 | async-start | bytes 4194304 | tf_op jit(solution)/shard_map/all_to_all | solution.py:156
  171.5 3.5 %fusion.12 = f32[512,512]{1,0:T(8,128)S(1)} fusion(bf16[1,2048,512]{2,1,0:T(8,128)(2,1)} %param.30, bf16[64,8,2048]{2,1,0:T(8,128)(2,1)} %all-to-all-done.1), kind=kOutput, calls=%fused_computation.22 | convolution fusion | flops 1073741824 | bytes 5242880 | tf_op jit(solution)/shard_map/dot_general | solution.py:56
  174.9 6.0 %fusion = bf16[64,8,2048]{2,1,0:T(8,128)(2,1)} fusion(bf16[1,512,2048]{2,1,0:T(8,128)(2,1)S(1)} %copy-done, bf16[1,2048,512]{2,1,0:T(8,128)(2,1)} %param.31, bf16[64,8,2048]{2,1,0:T(8,128)(2,1)} %all-to-all-done.1, f32[512,512]{1,0:T(8,128)S(1)} %fusion.12), kind=kOutput, calls=%fused_computation.8 | convolution fusion | flops 2150105088 | bytes 9437184 | tf_op jit(solution)/shard_map/dot_general | solution.py:59
  180.9 41.7 %all-to-all-done.4 = bf16[64,8,2048]{2,1,0:T(8,128)(2,1)} async-done(((bf16[64,8,2048]{2,1,0:T(8,128)(2,1)}), bf16[64,8,2048]{2,1,0:T(8,128)(2,1)}, u32[]{:S(2)}, u32[]{:S(2)}) %all-to-all-start.4) | async-done | bytes 2097184 | tf_op jit(solution)/shard_map/all_to_all | solution.py:156
  222.6 5.6 %all-to-all-start.2 = ((bf16[64,8,2048]{2,1,0:T(8,128)(2,1)}), bf16[64,8,2048]{2,1,0:T(8,128)(2,1)}, u32[]{:S(2)}, u32[]{:S(2)}) async-start(bf16[64,8,2048]{2,1,0:T(8,128)(2,1)} %fusion), calls=%async_computation.2 | async-start | bytes 4194304 | tf_op jit(solution)/shard_map/all_to_all | solution.py:156
  228.4 0.4 fusion.175
  228.9 0.4 fusion.174
  229.4 0.1 copy.40
  229.6 4.2 %gather_fusion.3 = bf16[256,2048]{1,0:T(8,128)(2,1)S(1)} fusion(bf16[512,2048]{1,0:T(8,128)(2,1)} %bitcast.23, s32[1024]{0:T(1024)S(1)} %pad_clamp_fusion), kind=kCustom, calls=%fused_computation.3.clone | custom fusion | bytes 2098176 | tf_op jit(solution)/shard_map/jit(_take)/gather | solution.py:86
  233.8 1.6 select_convert_fusion
  235.4 3.5 %reshape.233 = f32[128,2,2048]{2,1,0:T(2,128)} reshape(f32[256,2048]{1,0:T(8,128)} %select_convert_fusion) | data formatting | bytes 4194304 | tf_op jit(solution)/shard_map/convert_element_type | solution.py:89
  238.9 40.5 %all-to-all-done.2 = bf16[64,8,2048]{2,1,0:T(8,128)(2,1)} async-done(((bf16[64,8,2048]{2,1,0:T(8,128)(2,1)}), bf16[64,8,2048]{2,1,0:T(8,128)(2,1)}, u32[]{:S(2)}, u32[]{:S(2)}) %all-to-all-start.2) | async-done | bytes 2097184 | tf_op jit(solution)/shard_map/all_to_all | solution.py:156
  279.4 4.2 %gather_fusion.1 = bf16[256,2048]{1,0:T(8,128)(2,1)S(1)} fusion(bf16[512,2048]{1,0:T(8,128)(2,1)} %bitcast.16, s32[1024]{0:T(1024)S(1)} %pad_clamp_fusion.2), kind=kCustom, calls=%fused_computation.1.clone | custom fusion | bytes 2098176 | tf_op jit(solution)/shard_map/jit(_take)/gather | solution.py:86
  283.6 1.6 select_convert_fusion.1
  285.2 3.5 %reshape.232 = f32[128,2,2048]{2,1,0:T(2,128)} reshape(f32[256,2048]{1,0:T(8,128)} %select_convert_fusion.1) | data formatting | bytes 4194304 | tf_op jit(solution)/shard_map/convert_element_type | solution.py:89
  288.7 8.6 %multiply_reduce_fusion.1 = (f32[128,2048]{1,0:T(8,128)S(1)}, f32[128,2048]{1,0:T(8,128)S(1)}) fusion(f32[128,2,2048]{2,1,0:T(2,128)} %reshape.233, f32[128,2]{1,0:T(8,128)S(1)} %copy.40, f32[128,2,2048]{2,1,0:T(2,128)} %reshape.232, f32[128,2]{1,0:T(8,128)S(1)} %copy.35), kind=kLoop, calls=%fused_computation.30 | loop fusion | flops 1572864 | bytes 6293504 | tf_op jit(solution)/shard_map/reduce_sum | solution.py:89
  297.2 0.7 fusion.155
  297.9 0.8 multiply_reduce_fusion
  298.8 2.8 add_convert_fusion
  (66 shorter events, 0.9 us)
Async XLA Ops:
  0.0 118.2 %copy-start = (bf16[1,512,2048]{2,1,0:T(8,128)(2,1)S(1)}, bf16[1,512,2048]{2,1,0:T(8,128)(2,1)}, u32[]{:S(2)}) copy-start(bf16[1,512,2048]{2,1,0:T(8,128)(2,1)} %param.32) | copy-start | bytes 6291460
  0.0 13.5 %copy-start.14 = (f32[256]{0:T(256)S(1)}, f32[256]{0:T(256)}, u32[]{:S(2)}) copy-start(f32[256]{0:T(256)} %param.24) | copy-start | bytes 3076
  0.0 13.6 %copy-start.13 = (bf16[1,256,256]{2,1,0:T(8,128)(2,1)S(1)}, bf16[1,256,256]{2,1,0:T(8,128)(2,1)}, u32[]{:S(2)}) copy-start(bf16[1,256,256]{2,1,0:T(8,128)(2,1)} %param.23) | copy-start | bytes 393220
  0.9 11.5 %collective-permute-start = (bf16[15,256]{1,0:T(8,128)(2,1)S(1)}, bf16[15,256]{1,0:T(8,128)(2,1)S(1)}, u32[]{:S(2)}, u32[]{:S(2)}) collective-permute-start(bf16[15,256]{1,0:T(8,128)(2,1)S(1)} %slice.184), channel_id=1, source_target_pairs={{0,4},{4,8},{8,12},{12,16},{16,20},{20,24},{24,28},{28,32},{32,36}... | collective-permute-start | bytes 23048 | tf_op jit(solution)/shard_map/ppermute | solution.py:21
  3.5 7.4 %collective-permute-start.1 = (s32[15]{0:T(128)S(1)}, s32[15]{0:T(128)S(1)}, u32[]{:S(2)}, u32[]{:S(2)}) collective-permute-start(s32[15]{0:T(128)S(1)} %slice.186), channel_id=1, source_target_pairs={{0,4},{4,8},{8,12},{12,16},{16,20},{20,24},{24,28},{28,32},{32,36}... | collective-permute-start | bytes 188 | tf_op jit(solution)/shard_map/ppermute | solution.py:21
  18.9 13.9 %all-to-all-start = ((bf16[4,1,256,256]{3,2,1,0:T(8,128)(2,1)}), bf16[4,1,256,256]{3,2,1,0:T(8,128)(2,1)S(1)}, u32[]{:S(2)}, u32[]{:S(2)}) async-start(bf16[4,1,256,256]{3,2,1,0:T(8,128)(2,1)} %pad_maximum_fusion), calls=%async_computation | async-start | bytes 1048576 | tf_op jit(solution)/shard_map/all_to_all | solution.py:13
  36.9 1.4 copy-start.1
  36.9 0.7 copy-start.6
  37.0 0.8 copy-start.7
  38.3 1.0 copy-start.3
  45.8 15.2 %copy-start.12 = (pred[129]{0:T(512)(128)(4,1)S(1)}, pred[129]{0:T(512)(128)(4,1)}, u32[]{:S(2)}) copy-start(pred[129]{0:T(512)(128)(4,1)} %constant.119.clone.1) | copy-start | bytes 391
  45.8 63.3 %all-to-all-start.3 = ((bf16[64,8,2048]{2,1,0:T(8,128)(2,1)}), bf16[64,8,2048]{2,1,0:T(8,128)(2,1)}, u32[]{:S(2)}, u32[]{:S(2)}) async-start(bf16[64,8,2048]{2,1,0:T(8,128)(2,1)} %select_bitcast_fusion), calls=%async_computation.3 | async-start | bytes 4194304 | tf_op jit(solution)/shard_map/all_to_all | solution.py:158
  109.1 56.8 %all-to-all-start.1 = ((bf16[64,8,2048]{2,1,0:T(8,128)(2,1)}), bf16[64,8,2048]{2,1,0:T(8,128)(2,1)}, u32[]{:S(2)}, u32[]{:S(2)}) async-start(bf16[64,8,2048]{2,1,0:T(8,128)(2,1)} %select_bitcast_fusion.1), calls=%async_computation.1 | async-start | bytes 4194304 | tf_op jit(solution)/shard_map/all_to_all | solution.py:158
  165.9 56.8 %all-to-all-start.4 = ((bf16[64,8,2048]{2,1,0:T(8,128)(2,1)}), bf16[64,8,2048]{2,1,0:T(8,128)(2,1)}, u32[]{:S(2)}, u32[]{:S(2)}) async-start(bf16[64,8,2048]{2,1,0:T(8,128)(2,1)} %fusion.1), calls=%async_computation.4 | async-start | bytes 4194304 | tf_op jit(solution)/shard_map/all_to_all | solution.py:156
  180.9 47.4 %copy-start.8 = (s32[256,2]{0,1:T(2,128)S(1)}, s32[256,2]{0,1:T(2,128)}, u32[]{:S(2)}) copy-start(s32[256,2]{0,1:T(2,128)} %param.33) | copy-start | bytes 6148
  180.9 47.4 %copy-start.4 = (bf16[256,2048]{1,0:T(8,128)(2,1)S(1)}, bf16[256,2048]{1,0:T(8,128)(2,1)}, u32[]{:S(2)}) copy-start(bf16[256,2048]{1,0:T(8,128)(2,1)} %copy-done.3) | copy-start | bytes 3145732
  180.9 47.5 %copy-start.5 = (bf16[2048,64]{0,1:T(8,128)(2,1)S(1)}, bf16[2048,64]{0,1:T(8,128)(2,1)}, u32[]{:S(2)}) copy-start(bf16[2048,64]{0,1:T(8,128)(2,1)} %param.29) | copy-start | bytes 786436
  180.9 48.0 %copy-start.9 = (bf16[2048,4]{0,1:T(4,128)(2,1)S(1)}, bf16[2048,4]{0,1:T(4,128)(2,1)}, u32[]{:S(2)}) copy-start(bf16[2048,4]{0,1:T(4,128)(2,1)} %param.28) | copy-start | bytes 49156
  222.6 56.8 %all-to-all-start.2 = ((bf16[64,8,2048]{2,1,0:T(8,128)(2,1)}), bf16[64,8,2048]{2,1,0:T(8,128)(2,1)}, u32[]{:S(2)}, u32[]{:S(2)}) async-start(bf16[64,8,2048]{2,1,0:T(8,128)(2,1)} %fusion), calls=%async_computation.2 | async-start | bytes 4194304 | tf_op jit(solution)/shard_map/all_to_all | solution.py:156
  288.7 8.6 %copy-start.2 = (f32[256,2048]{1,0:T(8,128)S(1)}, f32[256,2048]{1,0:T(8,128)}, u32[]{:S(2)}) copy-start(f32[256,2048]{1,0:T(8,128)} %copy-done.1) | copy-start | bytes 6291460
  297.9 0.8 copy-start.10
  297.9 0.8 copy-start.11
